TPU v7x, 512 devices: a whole 4x8x8 slice. The times are simulated.
512 devices in a mesh: fs: 64 (over z, y), tp: 8 (over x, core).
Axes of the slice: x: 4, y: 8, z: 8, core: 2. Of those that a mesh axis runs over, the one named last changes fastest.
Arguments:
- tokens: bfloat16 [24576, 2048], P('fs', 'tp'), may hold values from -6 to 6
- outer_gate: bfloat16 [2048, 2048], P('fs', 'tp'), may hold values from -0.125 to 0.125
- inner_gate: bfloat16 [2048, 2048], P('fs', 'tp'), may hold values from -0.125 to 0.125
- mix_value: bfloat16 [2048, 2048], P('fs', 'tp'), may hold values from -0.125 to 0.125
- mix_taps: bfloat16 [3, 2048], P(None, 'tp'), may hold values from -3 to 3
- mix_out: bfloat16 [2048, 2048], P('tp', 'fs'), may hold values from -0.375 to 0.375
- mix_gain: bfloat16 [2048], P('tp'), may hold values from 0.099609375 to 1.8984375
- ffn_gate: bfloat16 [2048, 3072], P('fs', 'tp'), may hold values from -0.125 to 0.125
- ffn_value: bfloat16 [2048, 3072], P('fs', 'tp'), may hold values from -0.125 to 0.125
- gate_taps: bfloat16 [3, 3072], P(None, 'tp'), may hold values from -3 to 3
- value_taps: bfloat16 [3, 3072], P(None, 'tp'), may hold values from -3 to 3
- ffn_down: bfloat16 [3072, 2048], P('tp', 'fs'), may hold values from -0.3125 to 0.3125
- ffn_gain: bfloat16 [2048], P('tp'), may hold values from 0.099609375 to 1.8984375
Outputs:
- layer_out: bfloat16 [24576, 2048], P('fs', 'tp')
All inputs are finite; a program needn't handle non-finite values.
Results may differ from a plain program's by a relative error of at most 0.015.
Values may be sent and summed in bfloat16 or wider, within the bound.
A program may use at most 64 MiB of HBM per device.

v0:
```python
import jax
import jax.numpy as jnp
from jax import lax
from jax.sharding import PartitionSpec as P

SEQ_LEN = 128
residual_scale = 8.0**0.25
norm_epsilon = 1e-05


def copy_for_each(value, axis):
    copies = jnp.broadcast_to(value, (lax.axis_size(axis), *value.shape))
    return lax.all_to_all(copies, axis, split_axis=0, concat_axis=0, tiled=True)


def taken_together(value, axis):
    everything = copy_for_each(value, axis)
    return jnp.sum(everything, axis=0)


def in_one(arrays, axis):
    ends = [0]
    for a in arrays:
        ends.append(ends[-1] + a.size)
    subtotal = taken_together(jnp.concatenate([a.ravel() for a in arrays]), axis)
    return tuple((subtotal[b:e].reshape(a.shape) for a, b, e in zip(arrays, ends, ends[1:])))


def in_one_piece(arrays, axis, dim, along):
    both = jnp.concatenate(arrays, axis=along)
    filled, at, finished = (lax.all_gather(both, axis, axis=dim, tiled=True), 0, [])
    for a in arrays:
        finished.append(lax.slice_in_dim(filled, at, at + a.shape[along], axis=along))
        at += a.shape[along]
    return tuple(finished)


def laid_out(blocks, dim):
    blocks = jnp.moveaxis(blocks, 0, dim)
    dims = blocks.shape
    return blocks.reshape(*dims[:dim], dims[dim] * dims[dim + 1], *dims[dim + 2 :])


def collect(value, axis, dim):
    return laid_out(copy_for_each(value, axis), dim)


def split_up(value, dim, peers):
    before, after = (value.shape[:dim], value.shape[dim + 1 :])
    return jnp.moveaxis(value.reshape(*before, peers, -1, *after), dim, 0)


def sent_and_summed(value, axis, dim):
    peers = lax.axis_size(axis)
    blocks = lax.all_to_all(split_up(value, dim, peers), axis, 0, 0, tiled=True)
    return jnp.sum(blocks.astype(jnp.float32), axis=0)


def stored(values):
    return lax.optimization_barrier(values.astype(jnp.bfloat16)).astype(jnp.float32)


def shift_rows(values, offset):
    position = jnp.arange(values.shape[0]) % SEQ_LEN
    shifted = jnp.concatenate(
        [jnp.zeros((offset, values.shape[1]), values.dtype), values[:-offset]], axis=0
    )
    return jnp.where((position >= offset)[:, None], shifted, jnp.zeros_like(shifted))


def causal_taps(values, taps):
    weights = taps.astype(jnp.float32)
    return (
        values * weights[2]
        + shift_rows(values, 1) * weights[1]
        + shift_rows(values, 2) * weights[0]
    )


def fold_rows(whole, pieces):
    return tuple((jnp.dot(whole, piece, preferred_element_type=jnp.float32) for piece in pieces))


def norm_shares(prenorm, gain):
    width = prenorm.shape[1] * lax.axis_size("tp")
    row_sums = jnp.sum(prenorm, axis=1)
    row_squares = jnp.sum(prenorm * prenorm, axis=1)
    total, total_squares = in_one((row_sums, row_squares), "tp")
    mean = total / width
    spread = total_squares / width - mean * mean
    scaled = (prenorm - mean[:, None]) * lax.rsqrt(spread[:, None] + norm_epsilon)
    return (scaled * gain.astype(jnp.float32)).astype(jnp.bfloat16)


def body(
    tokens,
    outer_gate,
    inner_gate,
    mix_value,
    mix_taps,
    mix_out,
    mix_gain,
    ffn_gate,
    ffn_value,
    gate_taps,
    value_taps,
    ffn_down,
    ffn_gain,
):
    gate_whole, value_whole = in_one_piece((ffn_gate, ffn_value), "fs", 0, 1)
    whole_tokens = collect(tokens, "tp", 1)
    outer, inner, values = fold_rows(
        whole_tokens, in_one_piece((outer_gate, inner_gate, mix_value), "fs", 0, 1)
    )
    outer, inner, values = (stored(outer), stored(inner), stored(values))
    gated = (outer * causal_taps(inner * values, mix_taps)).astype(jnp.bfloat16)
    mixer_terms = jnp.dot(gated, collect(mix_out, "fs", 1), preferred_element_type=jnp.float32)
    mixer_branch = sent_and_summed(mixer_terms.astype(jnp.bfloat16), "tp", 1)
    first_own = norm_shares(residual_scale * tokens.astype(jnp.float32) + mixer_branch, mix_gain)
    first_whole = collect(first_own, "tp", 1)
    gate_up = jnp.dot(first_whole, gate_whole, preferred_element_type=jnp.float32)
    value_up = jnp.dot(first_whole, value_whole, preferred_element_type=jnp.float32)
    gate_up, value_up = (stored(gate_up), stored(value_up))
    hidden = (
        jax.nn.silu(causal_taps(gate_up, gate_taps)) * causal_taps(value_up, value_taps)
    ).astype(jnp.bfloat16)
    ffn_terms = jnp.dot(
        hidden,
        lax.all_gather(ffn_down, "fs", axis=1, tiled=True),
        preferred_element_type=jnp.float32,
    )
    ffn_branch = sent_and_summed(ffn_terms.astype(jnp.bfloat16), "tp", 1)
    return norm_shares(residual_scale * first_own.astype(jnp.float32) + ffn_branch, ffn_gain)


def solution(mesh):
    placed = (
        P("fs", "tp"),
        P("fs", "tp"),
        P("fs", "tp"),
        P("fs", "tp"),
        P(None, "tp"),
        P("tp", "fs"),
        P("tp"),
        P("fs", "tp"),
        P("fs", "tp"),
        P(None, "tp"),
        P(None, "tp"),
        P("tp", "fs"),
        P("tp"),
    )
    return jax.shard_map(body, mesh=mesh, in_specs=placed, out_specs=P("fs", "tp"), check_vma=False)
```

profile of v0, /device:TPU:1, one launch (start us, length us, event | category | flops | bytes accessed | tf_op | source)
XLA Modules:
  0.0 324.7 jit_solution(7652189762097484057)
XLA Ops:
  6.5 0.0 all-gather.4.cloned.1.call-start
  6.5 1.4 pad_maximum_fusion
  7.9 0.0 all-gather.4.cloned.1.call-update
  7.9 0.0 all-gather.6.cloned.1.call-start
  8.0 1.4 pad_maximum_fusion.1
  9.4 0.0 all-gather.6.cloned.1.call-update
  9.4 1.1 copy.25
  10.5 0.1 broadcast_in_dim.65
  10.6 0.0 copy-start.1
  10.6 29.8 %all_to_all.37 = bf16[8,384,256]{1,2,0:T(8,128)(2,1)S(1)} all-to-all(bf16[8,384,256]{1,2,0:T(8,128)(2,1)S(1)} %broadcast_in_dim.65), channel_id=1, replica_groups=mesh['fs'=64,'tp'=8] {'tp'}, dimensions={0} | all-to-all | bytes 3145728 | tf_op jit(solution)/shard_map/all_to_all | solution.py:13
  40.5 0.0 copy-done.1
  40.5 1.1 broadcast_in_dim.68
  41.6 12.7 %all-to-all-start.1 = ((bf16[64,256,32]{1,2,0:T(8,128)(2,1)}), bf16[64,256,32]{1,2,0:T(8,128)(2,1)S(1)}, u32[]{:S(2)}, u32[]{:S(2)}) async-start(bf16[64,256,32]{1,2,0:T(8,128)(2,1)} %broadcast_in_dim.68), calls=%async_computation.1 | async-start | bytes 2097152 | tf_op jit(solution)/shard_map/all_to_all | solution.py:13
  54.3 0.0 copy-done.2
  54.3 0.0 copy-start.7
  54.3 0.0 copy-start.9
  54.3 53.7 %all-gather.4.cloned.1.call-done = bf16[2048,768]{1,0:T(8,128)(2,1)} async-done(((bf16[32,768]{1,0:T(8,128)(2,1)}), bf16[2048,768]{1,0:T(8,128)(2,1)}) %all-gather.4.cloned.1.call-update) | async-done | bytes 3145744 | tf_op jit(solution)/shard_map/all_gather | solution.py:31
  108.0 2.0 fusion.11
  110.0 2.0 fusion.12
  112.0 2.0 fusion.10
  114.0 0.0 all-to-all-done.1
  114.0 0.0 copy-done.7
  114.0 0.0 copy-done.9
  114.0 1.0 convolution_convert_fusion.1
  115.1 1.3 copy.42
  116.3 8.6 %all-to-all-start.2 = ((bf16[8,384,256]{2,1,0:T(8,128)(2,1)}), bf16[8,384,256]{2,1,0:T(8,128)(2,1)S(1)}, u32[]{:S(2)}, u32[]{:S(2)}) async-start(bf16[8,384,256]{2,1,0:T(8,128)(2,1)} %bitcast.38), calls=%async_computation.2 | async-start | bytes 3145728 | tf_op jit(solution)/shard_map/all_to_all | solution.py:55
  124.9 0.0 all-gather.8.cloned.1.call-start
  125.0 0.7 all-gather.8.cloned.1.call-update
  125.7 19.8 %all-to-all-done.2 = bf16[8,384,256]{2,1,0:T(8,128)(2,1)S(1)} async-done(((bf16[8,384,256]{2,1,0:T(8,128)(2,1)}), bf16[8,384,256]{2,1,0:T(8,128)(2,1)S(1)}, u32[]{:S(2)}, u32[]{:S(2)}) %all-to-all-start.2) | async-done | bytes 1572896 | tf_op jit(solution)/shard_map/all_to_all | solution.py:55
  145.5 0.2 convert_reduce_fusion.1
  145.7 0.0 copy-done
  145.7 0.2 fusion.34
  145.9 0.6 broadcast_in_dim.69
  146.6 4.2 %all-to-all-start.3 = ((f32[8,1,768]{2,1,0:T(1,128)}), f32[8,1,768]{2,1,0:T(1,128)S(1)}, u32[]{:S(2)}, u32[]{:S(2)}) async-start(f32[8,1,768]{2,1,0:T(1,128)} %broadcast_in_dim.69), calls=%async_computation.3 | async-start | bytes 49152 | tf_op jit(solution)/shard_map/all_to_all | solution.py:13
  150.8 0.0 copy-done.12
  150.8 4.7 %all-to-all-done.3 = f32[8,1,768]{2,1,0:T(1,128)S(1)} async-done(((f32[8,1,768]{2,1,0:T(1,128)}), f32[8,1,768]{2,1,0:T(1,128)S(1)}, u32[]{:S(2)}, u32[]{:S(2)}) %all-to-all-start.3) | async-done | bytes 24608 | tf_op jit(solution)/shard_map/all_to_all | solution.py:13
  155.5 0.2 multiply_convert_fusion.2
  155.7 0.2 copy.28
  155.9 1.3 broadcast_in_dim.70
  157.2 4.3 %all-to-all-start.4 = ((bf16[8,384,256]{1,2,0:T(8,128)(2,1)}), bf16[8,384,256]{1,2,0:T(8,128)(2,1)S(1)}, u32[]{:S(2)}, u32[]{:S(2)}) async-start(bf16[8,384,256]{1,2,0:T(8,128)(2,1)} %broadcast_in_dim.70), calls=%async_computation.4 | async-start | bytes 3145728 | tf_op jit(solution)/shard_map/all_to_all | solution.py:13
  161.5 0.0 copy-done.3
  161.5 0.0 copy-done.4
  161.5 0.6 slice_reduce_fusion.2
  162.2 30.5 %all-gather.6.cloned.1.call-done = bf16[2048,768]{1,0:T(8,128)(2,1)} async-done(((bf16[32,768]{1,0:T(8,128)(2,1)}), bf16[2048,768]{1,0:T(8,128)(2,1)}) %all-gather.6.cloned.1.call-update) | async-done | bytes 3145744 | tf_op jit(solution)/shard_map/all_gather | solution.py:31
  192.7 0.0 all-to-all-done.4
  192.7 2.6 fusion.4
  195.3 0.0 copy-done.11
  195.4 1.0 fusion.7
  196.4 0.0 copy-start.5
  196.4 0.0 copy-start.6
  196.4 0.0 copy-start.8
  196.4 0.0 copy-start.10
  196.5 78.2 %all-gather.8.cloned.1.call-done = bf16[384,2048]{0,1:T(8,128)(2,1)} async-done(((bf16[384,32]{0,1:T(8,128)(2,1)}), bf16[384,2048]{0,1:T(8,128)(2,1)}) %all-gather.8.cloned.1.call-update) | async-done | bytes 1572880 | tf_op jit(solution)/shard_map/all_gather | solution.py:129
  274.7 0.0 copy-done.5
  274.7 0.0 copy-done.8
  274.7 2.9 convolution_convert_fusion
  277.6 0.1 copy.41
  277.7 29.6 %all_to_all.38 = bf16[8,384,256]{2,1,0:T(8,128)(2,1)S(1)} all-to-all(bf16[8,384,256]{2,1,0:T(8,128)(2,1)S(1)} %bitcast.45), channel_id=1, replica_groups=mesh['fs'=64,'tp'=8] {'tp'}, dimensions={0} | all-to-all | bytes 3145728 | tf_op jit(solution)/shard_map/all_to_all | solution.py:55
  307.3 0.2 convert_reduce_fusion
  307.5 0.2 fusion.35
  307.7 0.6 broadcast_in_dim.73
  308.3 4.3 %all-to-all-start.6 = ((f32[8,1,768]{2,1,0:T(1,128)}), f32[8,1,768]{2,1,0:T(1,128)S(1)}, u32[]{:S(2)}, u32[]{:S(2)}) async-start(f32[8,1,768]{2,1,0:T(1,128)} %broadcast_in_dim.73), calls=%async_computation.6 | async-start | bytes 49152 | tf_op jit(solution)/shard_map/all_to_all | solution.py:13
  312.6 4.7 %all-to-all-done.6 = f32[8,1,768]{2,1,0:T(1,128)S(1)} async-done(((f32[8,1,768]{2,1,0:T(1,128)}), f32[8,1,768]{2,1,0:T(1,128)S(1)}, u32[]{:S(2)}, u32[]{:S(2)}) %all-to-all-start.6) | async-done | bytes 24608 | tf_op jit(solution)/shard_map/all_to_all | solution.py:13
  317.4 0.9 multiply_convert_fusion.1
  (27 shorter events, 0.3 us)
Async XLA Ops:
  6.5 101.5 %all-gather.4.cloned.1.call-start = ((), (), s32[]{:S(2)}) async-start(), calls=%async_computation.7 | async-start | bytes 3194880 | tf_op jit(solution)/shard_map/all_gather | solution.py:31
  7.9 184.7 %all-gather.6.cloned.1.call-start = ((), (), s32[]{:S(2)}) async-start(), calls=%async_computation.8 | async-start | bytes 3194880 | tf_op jit(solution)/shard_map/all_gather | solution.py:31
  10.6 29.8 %copy-start.1 = (bf16[256,32]{0,1:T(8,128)(2,1)S(1)}, bf16[256,32]{0,1:T(8,128)(2,1)}, u32[]{:S(2)}) copy-start(bf16[256,32]{0,1:T(8,128)(2,1)} %param.18) | copy-start | bytes 49156
  40.5 13.8 %copy-start.2 = (bf16[3,256]{1,0:T(4,128)(2,1)S(1)}, bf16[3,256]{1,0:T(4,128)(2,1)}, u32[]{:S(2)}) copy-start(bf16[3,256]{1,0:T(4,128)(2,1)} %param.17) | copy-start | bytes 4612
  41.6 72.4 %all-to-all-start.1 = ((bf16[64,256,32]{1,2,0:T(8,128)(2,1)}), bf16[64,256,32]{1,2,0:T(8,128)(2,1)S(1)}, u32[]{:S(2)}, u32[]{:S(2)}) async-start(bf16[64,256,32]{1,2,0:T(8,128)(2,1)} %broadcast_in_dim.68), calls=%async_computation.1 | async-start | bytes 2097152 | tf_op jit(solution)/shard_map/all_to_all | solution.py:13
  54.3 59.7 %copy-start.7 = (pred[384]{0:T(512)(128)(4,1)}, pred[384]{0:T(512)(128)(4,1)S(1)}, u32[]{:S(2)}) copy-start(pred[384]{0:T(512)(128)(4,1)S(1)} %get-tuple-element.22) | copy-start | bytes 1156
  54.3 59.7 %copy-start.9 = (pred[384]{0:T(512)(128)(4,1)}, pred[384]{0:T(512)(128)(4,1)S(1)}, u32[]{:S(2)}) copy-start(pred[384]{0:T(512)(128)(4,1)S(1)} %get-tuple-element.23) | copy-start | bytes 1156
  116.3 29.2 %all-to-all-start.2 = ((bf16[8,384,256]{2,1,0:T(8,128)(2,1)}), bf16[8,384,256]{2,1,0:T(8,128)(2,1)S(1)}, u32[]{:S(2)}, u32[]{:S(2)}) async-start(bf16[8,384,256]{2,1,0:T(8,128)(2,1)} %bitcast.38), calls=%async_computation.2 | async-start | bytes 3145728 | tf_op jit(solution)/shard_map/all_to_all | solution.py:55
  124.9 20.8 %copy-start = (bf16[384,256]{1,0:T(8,128)(2,1)S(1)}, bf16[384,256]{1,0:T(8,128)(2,1)}, u32[]{:S(2)}) copy-start(bf16[384,256]{1,0:T(8,128)(2,1)} %param.13) | copy-start | bytes 589828
  124.9 25.9 %copy-start.12 = (bf16[256]{0:T(256)(128)(2,1)S(1)}, bf16[256]{0:T(256)(128)(2,1)}, u32[]{:S(2)}) copy-start(bf16[256]{0:T(256)(128)(2,1)} %param.19) | copy-start | bytes 1540
  124.9 149.7 %all-gather.8.cloned.1.call-start = ((), (), s32[]{:S(2)}) async-start(), calls=%async_computation.9 | async-start | bytes 1597440 | tf_op jit(solution)/shard_map/all_gather | solution.py:129
  146.6 8.9 %all-to-all-start.3 = ((f32[8,1,768]{2,1,0:T(1,128)}), f32[8,1,768]{2,1,0:T(1,128)S(1)}, u32[]{:S(2)}, u32[]{:S(2)}) async-start(f32[8,1,768]{2,1,0:T(1,128)} %broadcast_in_dim.69), calls=%async_computation.3 | async-start | bytes 49152 | tf_op jit(solution)/shard_map/all_to_all | solution.py:13
  157.2 4.3 %copy-start.3 = (bf16[3,384]{1,0:T(4,128)(2,1)S(1)}, bf16[3,384]{1,0:T(4,128)(2,1)}, u32[]{:S(2)}) copy-start(bf16[3,384]{1,0:T(4,128)(2,1)} %param.22) | copy-start | bytes 6916
  157.2 4.3 %copy-start.4 = (bf16[3,384]{1,0:T(4,128)(2,1)S(1)}, bf16[3,384]{1,0:T(4,128)(2,1)}, u32[]{:S(2)}) copy-start(bf16[3,384]{1,0:T(4,128)(2,1)} %param.23) | copy-start | bytes 6916
  157.2 35.5 %all-to-all-start.4 = ((bf16[8,384,256]{1,2,0:T(8,128)(2,1)}), bf16[8,384,256]{1,2,0:T(8,128)(2,1)S(1)}, u32[]{:S(2)}, u32[]{:S(2)}) async-start(bf16[8,384,256]{1,2,0:T(8,128)(2,1)} %broadcast_in_dim.70), calls=%async_computation.4 | async-start | bytes 3145728 | tf_op jit(solution)/shard_map/all_to_all | solution.py:13
  192.7 2.7 copy-start.11
  196.4 78.3 %copy-start.5 = (f32[384]{0:T(512)S(1)}, f32[384]{0:T(512)}, u32[]{:S(2)}) copy-start(f32[384]{0:T(512)} %get-tuple-element.25) | copy-start | bytes 4612
  196.4 78.3 %copy-start.6 = (f32[384]{0:T(512)S(1)}, f32[384]{0:T(512)}, u32[]{:S(2)}) copy-start(f32[384]{0:T(512)} %get-tuple-element.26) | copy-start | bytes 4612
  196.4 78.3 %copy-start.8 = (pred[384]{0:T(512)(128)(4,1)S(1)}, pred[384]{0:T(512)(128)(4,1)}, u32[]{:S(2)}) copy-start(pred[384]{0:T(512)(128)(4,1)} %copy-done.7) | copy-start | bytes 1156
  196.4 78.3 %copy-start.10 = (pred[384]{0:T(512)(128)(4,1)S(1)}, pred[384]{0:T(512)(128)(4,1)}, u32[]{:S(2)}) copy-start(pred[384]{0:T(512)(128)(4,1)} %copy-done.9) | copy-start | bytes 1156
  307.3 5.3 %copy-start.13 = (bf16[256]{0:T(256)(128)(2,1)S(1)}, bf16[256]{0:T(256)(128)(2,1)}, u32[]{:S(2)}) copy-start(bf16[256]{0:T(256)(128)(2,1)} %param.25) | copy-start | bytes 1540
  308.3 9.0 %all-to-all-start.6 = ((f32[8,1,768]{2,1,0:T(1,128)}), f32[8,1,768]{2,1,0:T(1,128)S(1)}, u32[]{:S(2)}, u32[]{:S(2)}) async-start(f32[8,1,768]{2,1,0:T(1,128)} %broadcast_in_dim.73), calls=%async_computation.6 | async-start | bytes 49152 | tf_op jit(solution)/shard_map/all_to_all | solution.py:13
Sparse Core Ops, SparseCore 0:
  10.3 97.6 all-gather.3
  111.0 81.5 all-gather.5
  195.7 78.9 all-gather.7
where the time goes:
time: 326 us; the launch traced here: 325 us
  waiting for transfers between devices  192 us (59%)
  blocking collectives  59.4 us (18%)
  starting transfers between devices  34.1 us (10%)
  matrix products  13.4 us (4%)
  between operations  13.4 us (4%)
  local copies, waits for them, and re-layouts  7.32 us (2%)
  other arithmetic  4.73 us (1%)
    all_gather x2, waiting for transfers between devices, in_one_piece(): lax.all_gather(both, axis, axis=dim, tiled=True)  84.2 us
    all_gather x1, waiting for transfers between devices, body(): lax.all_gather(ffn_down, 'fs', axis=1, tiled=True)  78.2 us
    all_to_all x1, blocking collectives, copy_for_each(): return lax.all_to_all(copies, axis, split_axis=0, concat_axis=0, tiled=True)  29.8 us
    all_to_all x1, blocking collectives, sent_and_summed(): blocks = lax.all_to_all(split_up(value, dim, peers), axis, 0, 0, tiled=True)  29.6 us
    all_to_all x4, starting transfers between devices, copy_for_each(): return lax.all_to_all(copies, axis, split_axis=0, concat_axis=0, tiled=True)  25.5 us
    all_to_all x1, waiting for transfers between devices, sent_and_summed(): blocks = lax.all_to_all(split_up(value, dim, peers), axis, 0, 0, tiled=True)  19.8 us
    all_to_all x4, waiting for transfers between devices, copy_for_each(): return lax.all_to_all(copies, axis, split_axis=0, concat_axis=0, tiled=True)  9.4 us
    all_to_all x1, starting transfers between devices, sent_and_summed(): blocks = lax.all_to_all(split_up(value, dim, peers), axis, 0, 0, tiled=True)  8.57 us
  transfers between devices with their start and end apart: 8, of which 6 were waited for; matrix products, arithmetic and copies ran while one was open for 6% of the time, Pallas kernels for 0%

commit v1 on v0

--- a/solution.py
+++ b/solution.py
@@ -6,6 +6,29 @@
 SEQ_LEN = 128
 residual_scale = 8.0**0.25
 norm_epsilon = 1e-05
+
+
+def in_order(blocks, dim):
+    lengths = list(blocks.shape[1:])
+    lengths[dim] *= blocks.shape[0]
+    return jnp.moveaxis(blocks, 0, dim).reshape(lengths)
+
+
+def collected_by_bits(x, axis):
+    devices, place = (lax.axis_size(axis), lax.axis_index(axis))
+    blocks, bit = (x[None], 1)
+    while bit < devices:
+        received = lax.ppermute(blocks, axis, [(i, i ^ bit) for i in range(devices)])
+        low = place & bit == 0
+        blocks = jnp.concatenate(
+            [jnp.where(low, blocks, received), jnp.where(low, received, blocks)]
+        )
+        bit *= 2
+    return blocks
+
+
+def collect_2(shard, axis, dim):
+    return in_order(collected_by_bits(shard, axis), dim)
 
 
 def copy_for_each(value, axis):
@@ -124,11 +147,7 @@
     hidden = (
         jax.nn.silu(causal_taps(gate_up, gate_taps)) * causal_taps(value_up, value_taps)
     ).astype(jnp.bfloat16)
-    ffn_terms = jnp.dot(
-        hidden,
-        lax.all_gather(ffn_down, "fs", axis=1, tiled=True),
-        preferred_element_type=jnp.float32,
-    )
+    ffn_terms = jnp.dot(hidden, collect_2(ffn_down, "fs", 1), preferred_element_type=jnp.float32)
     ffn_branch = sent_and_summed(ffn_terms.astype(jnp.bfloat16), "tp", 1)
     return norm_shares(residual_scale * first_own.astype(jnp.float32) + ffn_branch, ffn_gain)
 

time: 326 us -> 287 us (0.88)
  the two profiles are of different devices: /device:TPU:1 before, /device:TPU:56 now
where the time goes in v1:
time: 287 us; the launch traced here: 286 us
  waiting for transfers between devices  134 us (47%)
  starting transfers between devices  60.6 us (21%)
  blocking collectives  51.5 us (18%)
  matrix products  13.9 us (5%)
  between operations  13.9 us (5%)
  local copies, waits for them, and re-layouts  6.68 us (2%)
  other arithmetic  4.79 us (2%)
    ppermute x6, waiting for transfers between devices, collected_by_bits(): lax.ppermute(blocks, axis, [(i, i ^ bit) for i in range(devices)])  92.1 us
    all_gather x2, waiting for transfers between devices, in_one_piece(): lax.all_gather(both, axis, axis=dim, tiled=True)  36.9 us
    all_to_all x4, starting transfers between devices, copy_for_each(): return lax.all_to_all(copies, axis, split_axis=0, concat_axis=0, tiled=True)  28.3 us
    ppermute x6, starting transfers between devices, collected_by_bits(): lax.ppermute(blocks, axis, [(i, i ^ bit) for i in range(devices)])  27.9 us
    all_to_all x1, blocking collectives, sent_and_summed(): blocks = lax.all_to_all(split_up(value, dim, peers), axis, 0, 0, tiled=True)  25.8 us
    all_to_all x1, blocking collectives, copy_for_each(): return lax.all_to_all(copies, axis, split_axis=0, concat_axis=0, tiled=True)  25.7 us
    dot_general x3, matrix products, fold_rows(): jnp.dot(whole, piece, preferred_element_type=jnp.float32)  5.91 us
  transfers between devices with their start and end apart: 13, of which 8 were waited for; matrix products, arithmetic and copies ran while one was open for 5% of the time, Pallas kernels for 0%

profile of v1, /device:TPU:56, one launch (start us, length us, event | category | flops | bytes accessed | tf_op | source)
XLA Modules:
  0.0 285.9 jit_solution(9932793783260116492)
XLA Ops:
  6.5 0.0 all-gather.3.cloned.1.call-start
  6.5 1.4 pad_maximum_fusion.5
  7.9 0.0 all-gather.3.cloned.1.call-update
  7.9 1.1 copy.25
  9.0 0.1 broadcast_in_dim.68
  9.2 0.0 copy-start.4
  9.2 25.7 %all_to_all.37 = bf16[8,384,256]{1,2,0:T(8,128)(2,1)S(1)} all-to-all(bf16[8,384,256]{1,2,0:T(8,128)(2,1)S(1)} %broadcast_in_dim.68), channel_id=1, replica_groups=mesh['fs'=64,'tp'=8] {'tp'}, dimensions={0} | all-to-all | bytes 3145728 | tf_op jit(solution)/shard_map/all_to_all | solution.py:36
  34.9 0.0 copy-start.5
  34.9 1.1 broadcast_in_dim.71
  36.0 15.9 %all-to-all-start.1 = ((bf16[64,256,32]{1,2,0:T(8,128)(2,1)}), bf16[64,256,32]{1,2,0:T(8,128)(2,1)S(1)}, u32[]{:S(2)}, u32[]{:S(2)}) async-start(bf16[64,256,32]{1,2,0:T(8,128)(2,1)} %broadcast_in_dim.71), calls=%async_computation.1 | async-start | bytes 2097152 | tf_op jit(solution)/shard_map/all_to_all | solution.py:36
  51.9 0.0 all-gather.5.cloned.1.call-start
  52.0 0.6 pad_maximum_fusion.6
  52.6 0.1 all-gather.5.cloned.1.call-update
  52.7 3.4 %collective-permute-start = (bf16[1,384,32]{1,2,0:T(8,128)(2,1)S(1)}, bf16[1,384,32]{1,2,0:T(8,128)(2,1)S(1)}, u32[]{:S(2)}, u32[]{:S(2)}) collective-permute-start(bf16[1,384,32]{1,2,0:T(8,128)(2,1)S(1)} %bitcast.57), channel_id=1, source_target_pairs={{0,8},{8,0},{16,24},{24,16},{32,40},{40,32},{48,56},{56,48},{64,72... | collective-permute-start | bytes 73736 | tf_op jit(solution)/shard_map/ppermute | solution.py:21
  56.1 19.5 %collective-permute-done = bf16[1,384,32]{1,2,0:T(8,128)(2,1)S(1)} collective-permute-done((bf16[1,384,32]{1,2,0:T(8,128)(2,1)S(1)}, bf16[1,384,32]{1,2,0:T(8,128)(2,1)S(1)}, u32[]{:S(2)}, u32[]{:S(2)}) %collective-permute-start) | collective-permute-done | bytes 24608 | tf_op jit(solution)/shard_map/ppermute | solution.py:21
  75.7 36.9 %all-gather.3.cloned.1.call-done = bf16[2048,768]{1,0:T(8,128)(2,1)} async-done(((bf16[32,768]{1,0:T(8,128)(2,1)}), bf16[2048,768]{1,0:T(8,128)(2,1)}) %all-gather.3.cloned.1.call-update) | async-done | bytes 3145744 | tf_op jit(solution)/shard_map/all_gather | solution.py:54
  112.6 2.0 fusion.11
  114.5 2.0 fusion.12
  116.5 2.0 fusion.10
  118.6 0.0 all-to-all-done.1
  118.6 1.1 convolution_convert_fusion.1
  119.6 1.2 copy.42
  120.9 4.4 %all-to-all-start.2 = ((bf16[8,384,256]{2,1,0:T(8,128)(2,1)}), bf16[8,384,256]{2,1,0:T(8,128)(2,1)S(1)}, u32[]{:S(2)}, u32[]{:S(2)}) async-start(bf16[8,384,256]{2,1,0:T(8,128)(2,1)} %bitcast.44), calls=%async_computation.2 | async-start | bytes 3145728 | tf_op jit(solution)/shard_map/all_to_all | solution.py:78
  125.3 3.7 %collective-permute-start.1 = (bf16[2,384,32]{1,2,0:T(8,128)(2,1)S(1)}, bf16[2,384,32]{1,2,0:T(8,128)(2,1)S(1)}, u32[]{:S(2)}, u32[]{:S(2)}) collective-permute-start(bf16[2,384,32]{1,2,0:T(8,128)(2,1)S(1)} %pad_maximum_fusion.7), channel_id=1, source_target_pairs={{0,16},{8,24},{16,0},{24,8},{32,48},{40,56},{48,32},{56,40},{64,80... | collective-permute-start | bytes 147464 | tf_op jit(solution)/shard_map/ppermute | solution.py:21
  129.0 4.6 %collective-permute-done.1 = bf16[2,384,32]{1,2,0:T(8,128)(2,1)S(1)} collective-permute-done((bf16[2,384,32]{1,2,0:T(8,128)(2,1)S(1)}, bf16[2,384,32]{1,2,0:T(8,128)(2,1)S(1)}, u32[]{:S(2)}, u32[]{:S(2)}) %collective-permute-start.1) | collective-permute-done | bytes 49184 | tf_op jit(solution)/shard_map/ppermute | solution.py:21
  133.6 5.5 %collective-permute-start.2 = (bf16[4,384,32]{1,2,0:T(8,128)(2,1)S(1)}, bf16[4,384,32]{1,2,0:T(8,128)(2,1)S(1)}, u32[]{:S(2)}, u32[]{:S(2)}) collective-permute-start(bf16[4,384,32]{1,2,0:T(8,128)(2,1)S(1)} %pad_maximum_fusion.4), channel_id=1, source_target_pairs={{0,32},{8,40},{16,48},{24,56},{32,0},{40,8},{48,16},{56,24},{64,96... | collective-permute-start | bytes 294920 | tf_op jit(solution)/shard_map/ppermute | solution.py:21
  139.1 6.3 %collective-permute-done.2 = bf16[4,384,32]{1,2,0:T(8,128)(2,1)S(1)} collective-permute-done((bf16[4,384,32]{1,2,0:T(8,128)(2,1)S(1)}, bf16[4,384,32]{1,2,0:T(8,128)(2,1)S(1)}, u32[]{:S(2)}, u32[]{:S(2)}) %collective-permute-start.2) | collective-permute-done | bytes 98336 | tf_op jit(solution)/shard_map/ppermute | solution.py:21
  145.5 0.0 copy-start
  145.5 2.8 collective-permute-start.3
  148.3 5.0 %collective-permute-done.3 = bf16[8,384,32]{1,2,0:T(8,128)(2,1)S(1)} collective-permute-done((bf16[8,384,32]{1,2,0:T(8,128)(2,1)S(1)}, bf16[8,384,32]{1,2,0:T(8,128)(2,1)S(1)}, u32[]{:S(2)}, u32[]{:S(2)}) %collective-permute-start.3) | collective-permute-done | bytes 196640 | tf_op jit(solution)/shard_map/ppermute | solution.py:21
  153.4 0.1 broadcast_select_fusion.5
  153.4 0.0 all-to-all-done.2
  153.4 0.2 convert_reduce_fusion.1
  153.7 0.0 copy-done
  153.7 0.2 fusion.34
  153.9 0.6 broadcast_in_dim.72
  154.5 4.2 %all-to-all-start.3 = ((f32[8,1,768]{2,1,0:T(1,128)}), f32[8,1,768]{2,1,0:T(1,128)S(1)}, u32[]{:S(2)}, u32[]{:S(2)}) async-start(f32[8,1,768]{2,1,0:T(1,128)} %broadcast_in_dim.72), calls=%async_computation.3 | async-start | bytes 49152 | tf_op jit(solution)/shard_map/all_to_all | solution.py:36
  158.8 5.6 %collective-permute-start.4 = (bf16[16,384,32]{1,2,0:T(8,128)(2,1)S(1)}, bf16[16,384,32]{1,2,0:T(8,128)(2,1)S(1)}, u32[]{:S(2)}, u32[]{:S(2)}) collective-permute-start(bf16[16,384,32]{1,2,0:T(8,128)(2,1)S(1)} %pad_maximum_fusion.2), channel_id=1, source_target_pairs={{0,128},{8,136},{16,144},{24,152},{32,160},{40,168},{48,176},{56,1... | collective-permute-start | bytes 1179656 | tf_op jit(solution)/shard_map/ppermute | solution.py:21
  164.4 0.0 all-to-all-done.3
  164.4 0.2 multiply_convert_fusion.2
  164.6 0.2 copy.28
  164.8 1.3 broadcast_in_dim.73
  166.1 4.8 %all-to-all-start.4 = ((bf16[8,384,256]{1,2,0:T(8,128)(2,1)}), bf16[8,384,256]{1,2,0:T(8,128)(2,1)}, u32[]{:S(2)}, u32[]{:S(2)}) async-start(bf16[8,384,256]{1,2,0:T(8,128)(2,1)} %broadcast_in_dim.73), calls=%async_computation.4 | async-start | bytes 3145728 | tf_op jit(solution)/shard_map/all_to_all | solution.py:36
  170.9 0.0 copy-start.7
  170.9 18.6 %collective-permute-done.4 = bf16[16,384,32]{1,2,0:T(8,128)(2,1)S(1)} collective-permute-done((bf16[16,384,32]{1,2,0:T(8,128)(2,1)S(1)}, bf16[16,384,32]{1,2,0:T(8,128)(2,1)S(1)}, u32[]{:S(2)}, u32[]{:S(2)}) %collective-permute-start.4) | collective-permute-done | bytes 393248 | tf_op jit(solution)/shard_map/ppermute | solution.py:21
  189.5 0.1 broadcast_select_fusion.3
  189.7 0.1 pad_maximum_fusion.1
  189.8 7.0 %collective-permute-start.5 = (bf16[32,384,32]{1,2,0:T(8,128)(2,1)S(1)}, bf16[32,384,32]{1,2,0:T(8,128)(2,1)S(1)}, u32[]{:S(2)}, u32[]{:S(2)}) collective-permute-start(bf16[32,384,32]{1,2,0:T(8,128)(2,1)S(1)} %pad_maximum_fusion.1), channel_id=1, source_target_pairs={{0,256},{8,264},{16,272},{24,280},{32,288},{40,296},{48,304},{56,3... | collective-permute-start | bytes 2359304 | tf_op jit(solution)/shard_map/ppermute | solution.py:21
  196.8 38.1 %collective-permute-done.5 = bf16[32,384,32]{1,2,0:T(8,128)(2,1)S(1)} collective-permute-done((bf16[32,384,32]{1,2,0:T(8,128)(2,1)S(1)}, bf16[32,384,32]{1,2,0:T(8,128)(2,1)S(1)}, u32[]{:S(2)}, u32[]{:S(2)}) %collective-permute-start.5) | collective-permute-done | bytes 786464 | tf_op jit(solution)/shard_map/ppermute | solution.py:21
  234.9 0.2 broadcast_select_fusion.1
  235.1 0.2 pad_maximum_fusion
  235.3 0.0 all-gather.5.cloned.1.call-done
  235.3 0.0 all-to-all-done.4
  235.3 3.0 %fusion.4 = bf16[384,384]{1,0:T(8,128)(2,1)S(1)} fusion(bf16[384,2048]{0,1:T(8,128)(2,1)} %bitcast.13, bf16[2048,768]{1,0:T(8,128)(2,1)} %all-gather.5.cloned.1.call-done), kind=kOutput, calls=%fused_computation.11 | convolution fusion | flops 604127232 | bytes 3440640 | tf_op jit(solution)/shard_map/dot_general | solution.py:144
  238.5 2.4 fusion.7
  241.0 1.5 convolution_convert_fusion
  242.5 0.1 copy.41
  242.6 25.8 %all_to_all.38 = bf16[8,384,256]{2,1,0:T(8,128)(2,1)S(1)} all-to-all(bf16[8,384,256]{2,1,0:T(8,128)(2,1)S(1)} %bitcast.51), channel_id=1, replica_groups=mesh['fs'=64,'tp'=8] {'tp'}, dimensions={0} | all-to-all | bytes 3145728 | tf_op jit(solution)/shard_map/all_to_all | solution.py:78
  268.4 0.2 convert_reduce_fusion
  268.7 0.2 fusion.35
  268.9 0.6 broadcast_in_dim.77
  269.5 3.3 %all-to-all-start.6 = ((f32[8,1,768]{2,1,0:T(1,128)}), f32[8,1,768]{2,1,0:T(1,128)S(1)}, u32[]{:S(2)}, u32[]{:S(2)}) async-start(f32[8,1,768]{2,1,0:T(1,128)} %broadcast_in_dim.77), calls=%async_computation.6 | async-start | bytes 49152 | tf_op jit(solution)/shard_map/all_to_all | solution.py:36
  272.9 5.3 %all-to-all-done.6 = f32[8,1,768]{2,1,0:T(1,128)S(1)} async-done(((f32[8,1,768]{2,1,0:T(1,128)}), f32[8,1,768]{2,1,0:T(1,128)S(1)}, u32[]{:S(2)}, u32[]{:S(2)}) %all-to-all-start.6) | async-done | bytes 24608 | tf_op jit(solution)/shard_map/all_to_all | solution.py:36
  278.2 0.9 multiply_convert_fusion.1
  (42 shorter events, 0.6 us)
Async XLA Ops:
  6.5 106.0 %all-gather.3.cloned.1.call-start = ((), (), s32[]{:S(2)}) async-start(), calls=%async_computation.7 | async-start | bytes 3194880 | tf_op jit(solution)/shard_map/all_gather | solution.py:54
  9.2 25.7 %copy-start.4 = (bf16[256,32]{0,1:T(8,128)(2,1)S(1)}, bf16[256,32]{0,1:T(8,128)(2,1)}, u32[]{:S(2)}) copy-start(bf16[256,32]{0,1:T(8,128)(2,1)} %param.18) | copy-start | bytes 49156
  34.9 17.1 %copy-start.1 = (bf16[32,384]{1,0:T(8,128)(2,1)S(1)}, bf16[32,384]{1,0:T(8,128)(2,1)}, u32[]{:S(2)}) copy-start(bf16[32,384]{1,0:T(8,128)(2,1)} %param.21) | copy-start | bytes 73732
  34.9 17.1 %copy-start.2 = (bf16[32,384]{1,0:T(8,128)(2,1)S(1)}, bf16[32,384]{1,0:T(8,128)(2,1)}, u32[]{:S(2)}) copy-start(bf16[32,384]{1,0:T(8,128)(2,1)} %param.20) | copy-start | bytes 73732
  34.9 17.8 %copy-start.3 = (bf16[384,32]{0,1:T(8,128)(2,1)S(1)}, bf16[384,32]{0,1:T(8,128)(2,1)}, u32[]{:S(2)}) copy-start(bf16[384,32]{0,1:T(8,128)(2,1)} %param.24) | copy-start | bytes 73732
  34.9 21.2 %copy-start.5 = (bf16[3,256]{1,0:T(4,128)(2,1)S(1)}, bf16[3,256]{1,0:T(4,128)(2,1)}, u32[]{:S(2)}) copy-start(bf16[3,256]{1,0:T(4,128)(2,1)} %param.17) | copy-start | bytes 4612
  36.0 82.5 %all-to-all-start.1 = ((bf16[64,256,32]{1,2,0:T(8,128)(2,1)}), bf16[64,256,32]{1,2,0:T(8,128)(2,1)S(1)}, u32[]{:S(2)}, u32[]{:S(2)}) async-start(bf16[64,256,32]{1,2,0:T(8,128)(2,1)} %broadcast_in_dim.71), calls=%async_computation.1 | async-start | bytes 2097152 | tf_op jit(solution)/shard_map/all_to_all | solution.py:36
  51.9 183.4 %all-gather.5.cloned.1.call-start = ((), (), s32[]{:S(2)}) async-start(), calls=%async_computation.8 | async-start | bytes 3194880 | tf_op jit(solution)/shard_map/all_gather | solution.py:54
  52.7 23.0 %collective-permute-start = (bf16[1,384,32]{1,2,0:T(8,128)(2,1)S(1)}, bf16[1,384,32]{1,2,0:T(8,128)(2,1)S(1)}, u32[]{:S(2)}, u32[]{:S(2)}) collective-permute-start(bf16[1,384,32]{1,2,0:T(8,128)(2,1)S(1)} %bitcast.57), channel_id=1, source_target_pairs={{0,8},{8,0},{16,24},{24,16},{32,40},{40,32},{48,56},{56,48},{64,72... | collective-permute-start | bytes 73736 | tf_op jit(solution)/shard_map/ppermute | solution.py:21
  120.9 27.4 %copy-start.9 = (bf16[256]{0:T(256)(128)(2,1)S(1)}, bf16[256]{0:T(256)(128)(2,1)}, u32[]{:S(2)}) copy-start(bf16[256]{0:T(256)(128)(2,1)} %param.19) | copy-start | bytes 1540
  120.9 32.6 %all-to-all-start.2 = ((bf16[8,384,256]{2,1,0:T(8,128)(2,1)}), bf16[8,384,256]{2,1,0:T(8,128)(2,1)S(1)}, u32[]{:S(2)}, u32[]{:S(2)}) async-start(bf16[8,384,256]{2,1,0:T(8,128)(2,1)} %bitcast.44), calls=%async_computation.2 | async-start | bytes 3145728 | tf_op jit(solution)/shard_map/all_to_all | solution.py:78
  125.3 8.3 %collective-permute-start.1 = (bf16[2,384,32]{1,2,0:T(8,128)(2,1)S(1)}, bf16[2,384,32]{1,2,0:T(8,128)(2,1)S(1)}, u32[]{:S(2)}, u32[]{:S(2)}) collective-permute-start(bf16[2,384,32]{1,2,0:T(8,128)(2,1)S(1)} %pad_maximum_fusion.7), channel_id=1, source_target_pairs={{0,16},{8,24},{16,0},{24,8},{32,48},{40,56},{48,32},{56,40},{64,80... | collective-permute-start | bytes 147464 | tf_op jit(solution)/shard_map/ppermute | solution.py:21
  133.6 11.9 %collective-permute-start.2 = (bf16[4,384,32]{1,2,0:T(8,128)(2,1)S(1)}, bf16[4,384,32]{1,2,0:T(8,128)(2,1)S(1)}, u32[]{:S(2)}, u32[]{:S(2)}) collective-permute-start(bf16[4,384,32]{1,2,0:T(8,128)(2,1)S(1)} %pad_maximum_fusion.4), channel_id=1, source_target_pairs={{0,32},{8,40},{16,48},{24,56},{32,0},{40,8},{48,16},{56,24},{64,96... | collective-permute-start | bytes 294920 | tf_op jit(solution)/shard_map/ppermute | solution.py:21
  145.5 8.2 %copy-start = (bf16[384,256]{1,0:T(8,128)(2,1)S(1)}, bf16[384,256]{1,0:T(8,128)(2,1)}, u32[]{:S(2)}) copy-start(bf16[384,256]{1,0:T(8,128)(2,1)} %param.13) | copy-start | bytes 589828
  145.5 7.9 %collective-permute-start.3 = (bf16[8,384,32]{1,2,0:T(8,128)(2,1)S(1)}, bf16[8,384,32]{1,2,0:T(8,128)(2,1)S(1)}, u32[]{:S(2)}, u32[]{:S(2)}) collective-permute-start(bf16[8,384,32]{1,2,0:T(8,128)(2,1)S(1)} %pad_maximum_fusion.3), channel_id=1, source_target_pairs={{0,64},{8,72},{16,80},{24,88},{32,96},{40,104},{48,112},{56,120},{... | collective-permute-start | bytes 589832 | tf_op jit(solution)/shard_map/ppermute | solution.py:21
  154.5 9.9 %all-to-all-start.3 = ((f32[8,1,768]{2,1,0:T(1,128)}), f32[8,1,768]{2,1,0:T(1,128)S(1)}, u32[]{:S(2)}, u32[]{:S(2)}) async-start(f32[8,1,768]{2,1,0:T(1,128)} %broadcast_in_dim.72), calls=%async_computation.3 | async-start | bytes 49152 | tf_op jit(solution)/shard_map/all_to_all | solution.py:36
  158.8 30.7 %collective-permute-start.4 = (bf16[16,384,32]{1,2,0:T(8,128)(2,1)S(1)}, bf16[16,384,32]{1,2,0:T(8,128)(2,1)S(1)}, u32[]{:S(2)}, u32[]{:S(2)}) collective-permute-start(bf16[16,384,32]{1,2,0:T(8,128)(2,1)S(1)} %pad_maximum_fusion.2), channel_id=1, source_target_pairs={{0,128},{8,136},{16,144},{24,152},{32,160},{40,168},{48,176},{56,1... | collective-permute-start | bytes 1179656 | tf_op jit(solution)/shard_map/ppermute | solution.py:21
  166.1 69.2 %all-to-all-start.4 = ((bf16[8,384,256]{1,2,0:T(8,128)(2,1)}), bf16[8,384,256]{1,2,0:T(8,128)(2,1)}, u32[]{:S(2)}, u32[]{:S(2)}) async-start(bf16[8,384,256]{1,2,0:T(8,128)(2,1)} %broadcast_in_dim.73), calls=%async_computation.4 | async-start | bytes 3145728 | tf_op jit(solution)/shard_map/all_to_all | solution.py:36
  170.9 25.8 %copy-start.6 = (bf16[3,384]{1,0:T(4,128)(2,1)S(1)}, bf16[3,384]{1,0:T(4,128)(2,1)}, u32[]{:S(2)}) copy-start(bf16[3,384]{1,0:T(4,128)(2,1)} %param.22) | copy-start | bytes 6916
  170.9 25.9 %copy-start.7 = (bf16[3,384]{1,0:T(4,128)(2,1)S(1)}, bf16[3,384]{1,0:T(4,128)(2,1)}, u32[]{:S(2)}) copy-start(bf16[3,384]{1,0:T(4,128)(2,1)} %param.23) | copy-start | bytes 6916
  189.8 45.1 %collective-permute-start.5 = (bf16[32,384,32]{1,2,0:T(8,128)(2,1)S(1)}, bf16[32,384,32]{1,2,0:T(8,128)(2,1)S(1)}, u32[]{:S(2)}, u32[]{:S(2)}) collective-permute-start(bf16[32,384,32]{1,2,0:T(8,128)(2,1)S(1)} %pad_maximum_fusion.1), channel_id=1, source_target_pairs={{0,256},{8,264},{16,272},{24,280},{32,288},{40,296},{48,304},{56,3... | collective-permute-start | bytes 2359304 | tf_op jit(solution)/shard_map/ppermute | solution.py:21
  235.3 3.1 %copy-start.8 = (bf16[2048,768]{1,0:T(8,128)(2,1)S(1)}, bf16[2048,768]{1,0:T(8,128)(2,1)}, u32[]{:S(2)}) copy-start(bf16[2048,768]{1,0:T(8,128)(2,1)} %all-gather.5.cloned.1.call-done) | copy-start | bytes 9437188
  268.4 4.4 %copy-start.10 = (bf16[256]{0:T(256)(128)(2,1)S(1)}, bf16[256]{0:T(256)(128)(2,1)}, u32[]{:S(2)}) copy-start(bf16[256]{0:T(256)(128)(2,1)} %param.25) | copy-start | bytes 1540
  269.5 8.7 %all-to-all-start.6 = ((f32[8,1,768]{2,1,0:T(1,128)}), f32[8,1,768]{2,1,0:T(1,128)S(1)}, u32[]{:S(2)}, u32[]{:S(2)}) async-start(f32[8,1,768]{2,1,0:T(1,128)} %broadcast_in_dim.77), calls=%async_computation.6 | async-start | bytes 49152 | tf_op jit(solution)/shard_map/all_to_all | solution.py:36
Sparse Core Ops, SparseCore 0:
  10.3 102.1 all-gather.2
  115.6 110.0 all-gather.4
